TPU v7x, 32 devices: a whole 2x2x4 slice. The times are simulated.
32 devices in a mesh: grp: 2 (over x), ep: 16 (over z, y, core).
Axes of the slice: x: 2, y: 2, z: 4, core: 2. Of those that a mesh axis runs over, the one named last changes fastest.
Arguments:
- queries: bfloat16 [32, 8, 128], P(('grp', 'ep')), parts along dimension 0, may hold values from -400 to 400
- fresh_token_key: bfloat16 [32, 2, 128], P(('grp', 'ep')), parts along dimension 0, may hold values from -6 to 6
- value_new: bfloat16 [32, 2, 128], P(('grp', 'ep')), parts along dimension 0, may hold values from -6 to 6
- forget_logit: float32 [32, 8], P(('grp', 'ep')), parts along dimension 0, may hold values from -8 to 8
- cache_keys: bfloat16 [32, 2, 4096, 128], P(('grp', 'ep')), parts along dimension 0, may hold values from -12 to 12
- cache_values: bfloat16 [32, 2, 4096, 128], P(('grp', 'ep')), parts along dimension 0, may hold values from -6 to 6
- cache_cumlog: float32 [32, 8, 4096], P(('grp', 'ep')), parts along dimension 0, may hold values from -572 to 0
- lengths: int32 [32], P(('grp', 'ep')), parts along dimension 0, may hold values from 1024 to 4096
- residual: bfloat16 [32, 2048], P('grp', 'ep'), parts along dimension 0, may hold values from -6 to 6
- out_weight: bfloat16 [1024, 2048], P(None, 'ep'), may hold values from -0.1875 to 0.1875
- norm_gain: float32 [2048], replicated, may hold values from 0.1 to 1.9
- expert_gate: bfloat16 [16, 704, 2048], P('ep'), may hold values from -0.125 to 0.125
- expert_up: bfloat16 [16, 704, 2048], P('ep'), may hold values from -0.125 to 0.125
- expert_down: bfloat16 [16, 704, 2048], P('ep'), may hold values from -0.21875 to 0.21875
- shared_gate: bfloat16 [1408, 2048], P('ep'), may hold values from -0.125 to 0.125
- shared_up: bfloat16 [1408, 2048], P('ep'), may hold values from -0.125 to 0.125
- shared_down: bfloat16 [1408, 2048], P(None, 'ep'), may hold values from -0.15625 to 0.15625
- routes: int32 [32, 6], P('grp'), parts along dimension 0, may hold values from 0 to 15, all different within a row; in each aligned block of 16 rows (0 to 15, 16 to 31, ...) at most 12 rows name the same one
- route_scores: float32 [32, 6], P('grp'), parts along dimension 0, may hold values from 0.05 to 1
Outputs:
- updated: bfloat16 [32, 2048], P('grp', 'ep'), parts along dimension 0
There are 2 independent parts, one for each index of `grp`. A program takes and returns all parts, laid end to end along the dimension named above; an argument that names none is the same for every part. Nothing has to cross between parts.
Inputs may be any that keep to these rules, and one draw needn't show every extreme that they name: `routes`: each row names 6 different experts; no expert is named by more than 12 rows of a part, a bound that some block reaches.
All inputs are finite; a program needn't handle non-finite values.
Results may differ from a plain program's by a relative error of at most 0.0068.
Values may be sent and summed in bfloat16 or wider, within the bound.
No kernel may reach another device: no remote copies, remote signals or barrier semaphores. Data moves between devices by JAX's collectives and lax.ppermute only.
A program may use at most 64 MiB of HBM per device.

v0:
```python
import jax
import jax.numpy as jnp
from jax import lax
from jax.sharding import PartitionSpec as P

CAP = 12
norm_eps = 1e-06
routed_scale = 2.5
contract_last = (((1,), (1,)), ((), ()))


def expert_hidden(row_block, gate_matrix, up_matrix):
    gate_part = lax.dot_general(
        row_block, gate_matrix, contract_last, preferred_element_type=jnp.float32
    )
    up_part = lax.dot_general(
        row_block, up_matrix, contract_last, preferred_element_type=jnp.float32
    )
    return (jax.nn.silu(gate_part) * up_part).astype(jnp.bfloat16)


def attention(
    queries,
    fresh_token_key,
    value_new,
    forget_logit,
    cache_keys,
    cache_values,
    cache_cumlog,
    lengths,
):
    batch_rows, head_count, head_size = queries.shape
    key_heads = cache_keys.shape[1]
    cache_span = cache_keys.shape[2]
    groups = head_count // key_heads
    inv_root = head_size ** (-0.5)
    grouped_heads = queries.reshape(batch_rows, key_heads, groups, head_size)
    scores = (
        jnp.einsum(
            "bkgd,bkpd->bkgp", grouped_heads, cache_keys, preferred_element_type=jnp.float32
        ).reshape(batch_rows, head_count, cache_span)
        * inv_root
    )
    positions = lax.broadcasted_iota(jnp.int32, (1, 1, cache_span), 2)
    last_pos = (lengths - 1)[:, None, None]
    latest = jnp.sum(jnp.where(positions == last_pos, cache_cumlog, 0.0), axis=2)
    log_gate = jax.nn.log_sigmoid(forget_logit)
    scores = scores + (latest + log_gate)[:, :, None] - cache_cumlog
    visible = positions < lengths[:, None, None]
    scores = jnp.where(visible, scores, -jnp.inf)
    own_score = (
        jnp.einsum(
            "tiuh,tih->tiu", grouped_heads, fresh_token_key, preferred_element_type=jnp.float32
        ).reshape(batch_rows, head_count)
        * inv_root
    )
    top_score = jnp.maximum(jnp.max(scores, axis=2), own_score)
    weights = jnp.where(visible, jnp.exp(scores - top_score[:, :, None]), 0.0)
    own_weight = jnp.exp(own_score - top_score)
    denominator = jnp.sum(weights, axis=2) + own_weight
    weighted = jnp.einsum(
        "bkgp,bkpd->bkgd",
        weights.astype(jnp.bfloat16).reshape(batch_rows, key_heads, groups, cache_span),
        cache_values,
        preferred_element_type=jnp.float32,
    )
    own_rounded = lax.optimization_barrier(own_weight.astype(jnp.bfloat16)).astype(jnp.float32)
    own_value = jnp.repeat(value_new, groups, axis=1).astype(jnp.float32)
    numerator = (
        weighted.reshape(batch_rows, head_count, head_size) + own_rounded[:, :, None] * own_value
    )
    return (
        (numerator / denominator[:, :, None])
        .astype(jnp.bfloat16)
        .reshape(batch_rows, head_count * head_size)
    )


def on_device(
    queries,
    fresh_token_key,
    value_new,
    forget_logit,
    cache_keys,
    cache_values,
    cache_cumlog,
    lengths,
    residual,
    out_weight,
    norm_gain,
    expert_gate,
    expert_up,
    expert_down,
    shared_gate,
    shared_up,
    shared_down,
    routes,
    route_scores,
):
    attended = attention(
        queries,
        fresh_token_key,
        value_new,
        forget_logit,
        cache_keys,
        cache_values,
        cache_cumlog,
        lengths,
    )
    mixed = jnp.dot(
        lax.all_gather(attended, "ep", axis=0, tiled=True),
        out_weight,
        preferred_element_type=jnp.float32,
    )
    stream = (residual.astype(jnp.float32) + mixed).astype(jnp.bfloat16)
    full_rows = lax.all_gather(stream, "ep", axis=1, tiled=True)
    rows_wide = full_rows.astype(jnp.float32)
    inv_rms = lax.rsqrt(jnp.mean(rows_wide * rows_wide, axis=1, keepdims=True) + norm_eps)
    normed = (rows_wide * inv_rms * norm_gain).astype(jnp.bfloat16)
    gate_weights = route_scores / jnp.sum(route_scores, axis=1, keepdims=True) * routed_scale
    shared_mid = expert_hidden(normed, shared_gate, shared_up)
    my_expert = lax.axis_index("ep")
    expert_hits = routes == my_expert
    is_member = jnp.sum(expert_hits.astype(jnp.int32), axis=1)
    slot_rank = jnp.cumsum(is_member) - 1
    slot_ids = lax.broadcasted_iota(jnp.int32, (CAP, 1), 0)
    selector = (is_member[None, :] == 1) & (slot_rank[None, :] == slot_ids)
    picked = jnp.dot(
        selector.astype(jnp.bfloat16), normed, preferred_element_type=jnp.float32
    ).astype(jnp.bfloat16)
    hidden = expert_hidden(picked, expert_gate[0], expert_up[0])
    expert_out = jnp.dot(hidden, expert_down[0], preferred_element_type=jnp.float32).astype(
        jnp.bfloat16
    )
    received = lax.all_to_all(expert_out[None], "ep", split_axis=2, concat_axis=0, tiled=True)
    expert_count = received.shape[0]
    expert_ids = lax.broadcasted_iota(jnp.int32, (1, 1, expert_count), 2)
    all_hits = routes[:, :, None] == expert_ids
    membership = jnp.sum(all_hits.astype(jnp.int32), axis=1)
    share_all = jnp.sum(jnp.where(all_hits, gate_weights[:, :, None], 0.0), axis=1)
    rank_all = jnp.cumsum(membership, axis=0) - 1
    slot_grid = lax.broadcasted_iota(jnp.int32, (1, 1, CAP), 2)
    slot_mask = (membership[:, :, None] == 1) & (rank_all[:, :, None] == slot_grid)
    combiner = jnp.where(slot_mask, share_all[:, :, None], 0.0).reshape(
        routes.shape[0], expert_count * CAP
    )
    flat_slots = received.reshape(expert_count * CAP, received.shape[2]).astype(jnp.float32)
    routed_part = jnp.dot(combiner, flat_slots, precision=lax.Precision.HIGHEST)
    shared_part = jnp.dot(
        lax.all_gather(shared_mid, "ep", axis=1, tiled=True),
        shared_down,
        preferred_element_type=jnp.float32,
    )
    return (stream.astype(jnp.float32) + routed_part + shared_part).astype(jnp.bfloat16)


def solution(mesh):
    placed = (
        P(("grp", "ep"), None, None),
        P(("grp", "ep"), None, None),
        P(("grp", "ep"), None, None),
        P(("grp", "ep"), None),
        P(("grp", "ep"), None, None, None),
        P(("grp", "ep"), None, None, None),
        P(("grp", "ep"), None, None),
        P(("grp", "ep")),
        P("grp", "ep"),
        P(None, "ep"),
        P(),
        P("ep", None, None),
        P("ep", None, None),
        P("ep", None, None),
        P("ep", None),
        P("ep", None),
        P(None, "ep"),
        P("grp", None),
        P("grp", None),
    )
    return jax.shard_map(
        on_device, mesh=mesh, in_specs=placed, out_specs=P("grp", "ep"), check_vma=False
    )
```

profile of v0, /device:TPU:0, one launch (start us, length us, event | category | flops | bytes accessed | tf_op | source)
XLA Modules:
  0.0 110.7 jit_solution(4193211708962261572)
XLA Ops:
  0.0 0.9 fusion.47
  1.8 0.7 convert_reduce_fusion.1
  2.5 0.7 bitcast_convert_fusion
  3.3 0.1 add_reduce_fusion
  3.4 2.3 %convolution_multiply_fusion = f32[2,4,4096]{2,1,0:T(4,128)S(1)} fusion(bf16[2,4,128]{2,1,0:T(4,128)(2,1)} %bitcast.100, bf16[1,2,4096,128]{3,2,1,0:T(8,128)(2,1)} %param.23), kind=kOutput, calls=%fused_computation | convolution fusion | flops 8421376 | bytes 2230272 | tf_op jit(solution)/shard_map/bkgd,bkpd->bkgp/dot_general | solution.py:39
  5.7 1.1 select_reduce_fusion
  6.8 0.7 fusion.52
  7.5 1.1 %fusion.59 = (f32[8]{0:T(128)S(1)}, f32[1,8,4096]{2,1,0:T(8,128)S(1)}) fusion(f32[1,8,4096]{2,1,0:T(8,128)} %param.25, f32[1,8,4096]{2,1,0:T(8,128)S(1)} %mul.103, f32[8]{0:T(128)S(1)} %fusion.52, pred[4096]{0:T(1024)(128)(4,1)S(1)} %iota_compare_fusion.3), kind=kLoop, calls=%fused_computation.78 | loop fusion | flops 131064 | bytes 397376 | tf_op jit(solution)/shard_map/reduce_max | solution.py:57
  8.6 0.2 fusion.34
  8.9 2.0 %fusion.12 = f32[2,4,128]{2,1,0:T(4,128)S(1)} fusion(bf16[2,4,4096]{2,1,0:T(4,128)(2,1)S(1)} %reshape.347, bf16[1,2,4096,128]{3,2,1,0:T(8,128)(2,1)} %param.24), kind=kOutput, calls=%fused_computation.10 | convolution fusion | flops 8388608 | bytes 2166784 | tf_op jit(solution)/shard_map/bkgp,bkpd->bkgd/dot_general | solution.py:61
  11.1 23.3 %all-gather = bf16[16,1,1024]{2,1,0:T(2,128)(2,1)S(1)} all-gather(bf16[1,1,1024]{2,1,0:T(2,128)(2,1)S(1)} %convert_bitcast_fusion), channel_id=1, replica_groups=mesh['grp'=2,'ep'=16] {'ep'}, dimensions={0}, use_global_device_ids=true | all-gather | bytes 34816 | tf_op jit(solution)/shard_map/all_gather | solution.py:111
  34.4 0.2 fusion.22
  34.5 17.6 %all_gather.10 = bf16[16,2048]{1,0:T(8,128)(2,1)S(1)} all-gather(bf16[16,128]{1,0:T(8,128)(2,1)S(1)} %fusion.22), channel_id=1, replica_groups=mesh['grp'=2,'ep'=16] {'ep'}, dimensions={1}, use_global_device_ids=true | all-gather | bytes 69632 | tf_op jit(solution)/shard_map/all_gather | solution.py:116
  52.1 0.1 fusion.28
  52.2 0.2 convolution_convert_fusion
  52.5 2.7 %fusion.4 = f32[12,704]{1,0:T(8,128)S(1)} fusion(bf16[12,2048]{1,0:T(8,128)(2,1)S(1)} %convolution_convert_fusion, bf16[1,704,2048]{2,1,0:T(8,128)(2,1)} %param.30), kind=kOutput, calls=%fused_computation.5 | convolution fusion | flops 34603008 | bytes 2966528 | tf_op jit(solution)/shard_map/dot_general | solution.py:13
  55.1 3.5 %fusion.9 = bf16[1,12,2048]{2,1,0:T(8,128)(2,1)S(1)} fusion(bf16[1,704,2048]{2,1,0:T(8,128)(2,1)S(1)} %copy-done, bf16[12,2048]{1,0:T(8,128)(2,1)S(1)} %convolution_convert_fusion, bf16[1,704,2048]{2,1,0:T(8,128)(2,1)} %param.31, f32[12,704]{1,0:T(8,128)S(1)} %fusion.4), kind=kOutput, calls=%fused_computation.9 | convolution fusion | flops 69281280 | bytes 5899264 | tf_op jit(solution)/shard_map/dot_general | solution.py:132
  58.6 2.0 %copy.42 = bf16[1,12,2048]{1,0,2:T(2,128)(2,1)} copy(bf16[1,12,2048]{2,1,0:T(8,128)(2,1)S(1)} %fusion.9) | data formatting | bytes 98304 | tf_op jit(solution)/shard_map/broadcast_in_dim | solution.py:135
  60.7 0.5 broadcast.203
  61.2 12.6 %reduce.5 = bf16[2048,12]{1,0:T(8,128)(2,1)S(1)} reduce(bf16[2048,1,12]{2,1,0:T(2,128)(2,1)} %bitcast.91, bf16[]{:T(256)} %broadcast.203), dimensions={1}, to_apply=%bitcast.76.reduce_sub_computation | reduce | bytes 98306
  73.8 1.6 %reshape.361 = bf16[16,2,768]{2,1,0:T(2,128)(2,1)} reshape(bf16[2048,12]{1,0:T(8,128)(2,1)S(1)} %reduce.5) | data formatting | bytes 98304
  75.3 3.5 %all-to-all-start = ((bf16[16,2,768]{2,1,0:T(2,128)(2,1)}), bf16[16,2,768]{2,1,0:T(2,128)(2,1)S(1)}, u32[]{:S(2)}, u32[]{:S(2)}) async-start(bf16[16,2,768]{2,1,0:T(2,128)(2,1)} %reshape.361), calls=%async_computation | async-start | bytes 98304 | tf_op jit(solution)/shard_map/all_to_all | solution.py:135
  79.1 1.2 %fusion.56 = f32[16,88]{1,0:T(8,128)S(1)} fusion(bf16[88,2048]{1,0:T(8,128)(2,1)} %param.33, bf16[16,2048]{1,0:T(8,128)(2,1)S(1)} %all_gather.10, f32[2048]{0:T(1024)S(1)} %copy-done.2, f32[16]{0:T(128)S(1)} %add_rsqrt_fusion), kind=kOutput, calls=%fused_computation.77 | convolution fusion | flops 5898240 | bytes 439872 | tf_op jit(solution)/shard_map/dot_general | solution.py:13
  80.3 1.2 %fusion.25 = bf16[1,88,16]{1,2,0:T(8,128)(2,1)S(1)} fusion(bf16[88,2048]{1,0:T(8,128)(2,1)} %param.34, f32[16,88]{1,0:T(8,128)S(1)} %fusion.56, bf16[16,2048]{1,0:T(8,128)(2,1)S(1)} %all_gather.10, f32[2048]{0:T(1024)S(1)} %copy-done.2, f32[16]{0:T(128)S(1)} %add_rsqrt_fusion), kind=kOutput, calls=%fused_computation.22 | convolution fusion | flops 5906688 | bytes 442688 | tf_op jit(solution)/shard_map/dot_general | solution.py:16
  81.6 21.8 %all-gather.1 = bf16[16,88,16]{1,2,0:T(8,128)(2,1)S(1)} all-gather(bf16[1,88,16]{1,2,0:T(8,128)(2,1)S(1)} %fusion.25), channel_id=1, replica_groups=mesh['grp'=2,'ep'=16] {'ep'}, dimensions={0}, use_global_device_ids=true | all-gather | bytes 47872 | tf_op jit(solution)/shard_map/all_gather | solution.py:150
  103.4 0.1 reshape.357
  103.6 1.1 %fusion.60 = f32[16,128]{1,0:T(8,128)S(1)} fusion(bf16[1408,16]{0,1:T(8,128)(2,1)S(1)} %reshape.357, bf16[1408,128]{1,0:T(8,128)(2,1)} %param.35), kind=kOutput, calls=%fused_computation.79 | convolution fusion | flops 5767168 | bytes 413696 | tf_op jit(solution)/shard_map/dot_general | solution.py:149
  104.7 0.2 fusion.32
  104.9 0.1 select_n.39
  105.0 2.5 %reshape.362 = bf16[2048,1,12]{2,1,0:T(2,128)(2,1)} reshape(bf16[16,2,768]{2,1,0:T(2,128)(2,1)S(1)} %all-to-all-done) | data formatting | bytes 98304
  107.5 2.3 %copy.43 = bf16[1,12,2048]{2,1,0:T(8,128)(2,1)S(1)} copy(bf16[1,12,2048]{1,0,2:T(2,128)(2,1)} %bitcast.92) | data formatting | bytes 98304 | tf_op jit(solution)/shard_map/all_to_all | solution.py:135
  109.9 0.8 fusion.23
  (44 shorter events, 1.0 us)
Async XLA Ops:
  0.0 55.1 %copy-start = (bf16[1,704,2048]{2,1,0:T(8,128)(2,1)S(1)}, bf16[1,704,2048]{2,1,0:T(8,128)(2,1)}, u32[]{:S(2)}) copy-start(bf16[1,704,2048]{2,1,0:T(8,128)(2,1)} %param.32) | copy-start | bytes 8650756
  0.0 34.4 %copy-start.1 = (bf16[1024,128]{1,0:T(8,128)(2,1)S(1)}, bf16[1024,128]{1,0:T(8,128)(2,1)}, u32[]{:S(2)}) copy-start(bf16[1024,128]{1,0:T(8,128)(2,1)} %param.28) | copy-start | bytes 786436
  0.0 34.4 %copy-start.5 = (bf16[16,128]{1,0:T(8,128)(2,1)S(1)}, bf16[16,128]{1,0:T(8,128)(2,1)}, u32[]{:S(2)}) copy-start(bf16[16,128]{1,0:T(8,128)(2,1)} %param.27) | copy-start | bytes 12292
  3.4 48.8 %copy-start.2 = (f32[2048]{0:T(1024)S(1)}, f32[2048]{0:T(1024)}, u32[]{:S(2)}) copy-start(f32[2048]{0:T(1024)} %param.29) | copy-start | bytes 24580
  58.6 20.2 %copy-start.3 = (s32[16,6]{0,1:T(8,128)S(1)}, s32[16,6]{0,1:T(8,128)}, u32[]{:S(2)}) copy-start(s32[16,6]{0,1:T(8,128)} %param.36) | copy-start | bytes 1156
  58.6 20.3 %copy-start.4 = (f32[16,6]{0,1:T(8,128)S(1)}, f32[16,6]{0,1:T(8,128)}, u32[]{:S(2)}) copy-start(f32[16,6]{0,1:T(8,128)} %param.37) | copy-start | bytes 1156
  75.3 29.7 %all-to-all-start = ((bf16[16,2,768]{2,1,0:T(2,128)(2,1)}), bf16[16,2,768]{2,1,0:T(2,128)(2,1)S(1)}, u32[]{:S(2)}, u32[]{:S(2)}) async-start(bf16[16,2,768]{2,1,0:T(2,128)(2,1)} %reshape.361), calls=%async_computation | async-start | bytes 98304 | tf_op jit(solution)/shard_map/all_to_all | solution.py:135
where the time goes:
time: 111 us
  blocking collectives  62.7 us (56%)
  other arithmetic  17.8 us (16%)
  matrix products  16.1 us (15%)
  local copies, waits for them, and re-layouts  9.72 us (9%)
  starting transfers between devices  3.5 us (3%)
    all_gather x1, blocking collectives, on_device(): lax.all_gather(attended, 'ep', axis=0, tiled=True)  23.3 us
    all_gather x1, blocking collectives, on_device(): lax.all_gather(shared_mid, 'ep', axis=1, tiled=True)  21.8 us
    all_gather x1, blocking collectives, on_device(): full_rows = lax.all_gather(stream, 'ep', axis=1, tiled=True)  17.6 us
    unnamed x2, other arithmetic  12.6 us
    unnamed x17, local copies, waits for them, and re-layouts  4.7 us
    dot_general x2, matrix products, expert_hidden(): lax.dot_general(row_block, gate_matrix, contract_last, preferred_element_...  3.89 us
    all_to_all x1, starting transfers between devices, on_device(): lax.all_to_all(expert_out[None], 'ep', split_axis=2, concat_axis=0, tiled...  3.5 us
    dot_general x1, matrix products, on_device(): jnp.dot(hidden, expert_down[0], preferred_element_type=jnp.float32)  3.49 us
  transfers between devices with their start and end apart: 1, of which 0 were waited for; matrix products, arithmetic and copies ran while one was open for 4% of the time, Pallas kernels for 0%

commit v1 on v0

--- a/solution.py
+++ b/solution.py
@@ -132,7 +132,12 @@
     expert_out = jnp.dot(hidden, expert_down[0], preferred_element_type=jnp.float32).astype(
         jnp.bfloat16
     )
-    received = lax.all_to_all(expert_out[None], "ep", split_axis=2, concat_axis=0, tiled=True)
+    received = jnp.concatenate(
+        lax.all_to_all(
+            jnp.stack(jnp.split(expert_out[None], lax.axis_size("ep"), axis=2)), "ep", 0, 0
+        ),
+        axis=0,
+    )
     expert_count = received.shape[0]
     expert_ids = lax.broadcasted_iota(jnp.int32, (1, 1, expert_count), 2)
     all_hits = routes[:, :, None] == expert_ids

time: 111 us -> 96.8 us (0.87)
  other arithmetic: 17.8 us -> 3.89 us
    unnamed x2 -> x1, other arithmetic: 12.6 us -> 0.03 us
    unnamed x17 -> x32, local copies, waits for them, and re-layouts: 4.7 us -> 9.07 us
    all_to_all x3 -> x0, local copies, waits for them, and re-layouts: 2.35 us -> none  [on_device(): lax.all_to_all(expert_out[None], 'ep', split_axis=2, concat_axis=0, tiled...]
    broadcast_in_dim x1 -> x0, local copies, waits for them, and re-layouts: 2.04 us -> none  [on_device(): expert_out[None]]
  transfers between devices with their start and end apart: 1 -> 1, of which waited for: 0 -> 0; matrix products, arithmetic and copies ran while one was open for 4% -> 3% of each run, Pallas kernels for 0% -> 0%
where the time goes in v1:
time: 96.8 us; the launch traced here: 96.4 us
  blocking collectives  62.7 us (65%)
  matrix products  15.2 us (16%)
  local copies, waits for them, and re-layouts  10.3 us (11%)
  other arithmetic  3.89 us (4%)
  starting transfers between devices  3.5 us (4%)
    all_gather x1, blocking collectives, on_device(): lax.all_gather(attended, 'ep', axis=0, tiled=True)  23.3 us
    all_gather x1, blocking collectives, on_device(): lax.all_gather(shared_mid, 'ep', axis=1, tiled=True)  21.8 us
    all_gather x1, blocking collectives, on_device(): full_rows = lax.all_gather(stream, 'ep', axis=1, tiled=True)  17.6 us
    unnamed x32, local copies, waits for them, and re-layouts  9.07 us
    dot_general x2, matrix products, expert_hidden(): lax.dot_general(row_block, gate_matrix, contract_last, preferred_element_...  3.89 us
    dot_general x1, matrix products, on_device(): jnp.dot(hidden, expert_down[0], preferred_element_type=jnp.float32)  3.53 us
    all_to_all x1, starting transfers between devices, on_device(): lax.all_to_all(jnp.stack(jnp.split(expert_out[None], lax.axis_size('ep'),...  3.5 us
    dot_general x1, matrix products, attention(): jnp.einsum('bkgd,bkpd->bkgp', grouped_heads, cache_keys, preferred_elemen...  2.27 us
  transfers between devices with their start and end apart: 1, of which 0 were waited for; matrix products, arithmetic and copies ran while one was open for 3% of the time, Pallas kernels for 0%

profile of v1, /device:TPU:0, one launch (start us, length us, event | category | flops | bytes accessed | tf_op | source)
XLA Modules:
  0.0 96.4 jit_solution(13771426093455704900)
XLA Ops:
  0.0 1.0 fusion.47
  1.1 2.3 %convolution_multiply_fusion = f32[2,4,4096]{2,1,0:T(4,128)S(1)} fusion(bf16[2,4,128]{2,1,0:T(4,128)(2,1)} %bitcast.148, bf16[1,2,4096,128]{3,2,1,0:T(8,128)(2,1)} %param.23), kind=kOutput, calls=%fused_computation | convolution fusion | flops 8421376 | bytes 2230272 | tf_op jit(solution)/shard_map/bkgd,bkpd->bkgp/dot_general | solution.py:39
  4.2 1.1 %select_reduce_fusion = f32[8]{0:T(128)S(1)} fusion(f32[1,8,4096]{2,1,0:T(8,128)} %param.25, pred[4096]{0:T(1024)(128)(4,1)S(1)} %iota_compare_fusion.2), kind=kLoop, calls=%fused_computation.31 | loop fusion | flops 65528 | bytes 135200 | tf_op jit(solution)/shard_map/reduce_sum | solution.py:46
  5.2 0.7 fusion.52
  5.9 1.1 %fusion.59 = (f32[8]{0:T(128)S(1)}, f32[1,8,4096]{2,1,0:T(8,128)S(1)}) fusion(f32[1,8,4096]{2,1,0:T(8,128)} %param.25, f32[1,8,4096]{2,1,0:T(8,128)S(1)} %mul.103, f32[8]{0:T(128)S(1)} %fusion.52, pred[4096]{0:T(1024)(128)(4,1)S(1)} %iota_compare_fusion.3), kind=kLoop, calls=%fused_computation.109 | loop fusion | flops 131064 | bytes 397376 | tf_op jit(solution)/shard_map/reduce_max | solution.py:57
  7.3 2.0 %fusion.12 = f32[2,4,128]{2,1,0:T(4,128)S(1)} fusion(bf16[2,4,4096]{2,1,0:T(4,128)(2,1)S(1)} %reshape.343, bf16[1,2,4096,128]{3,2,1,0:T(8,128)(2,1)} %param.24), kind=kOutput, calls=%fused_computation.10 | convolution fusion | flops 8388608 | bytes 2166784 | tf_op jit(solution)/shard_map/bkgp,bkpd->bkgd/dot_general | solution.py:61
  9.5 23.3 %all-gather = bf16[16,1,1024]{2,1,0:T(2,128)(2,1)S(1)} all-gather(bf16[1,1,1024]{2,1,0:T(2,128)(2,1)S(1)} %convert_bitcast_fusion), channel_id=1, replica_groups=mesh['grp'=2,'ep'=16] {'ep'}, dimensions={0}, use_global_device_ids=true | all-gather | bytes 34816 | tf_op jit(solution)/shard_map/all_gather | solution.py:111
  33.0 17.6 %all_gather.10 = bf16[16,2048]{1,0:T(8,128)(2,1)S(1)} all-gather(bf16[16,128]{1,0:T(8,128)(2,1)S(1)} %fusion.22), channel_id=1, replica_groups=mesh['grp'=2,'ep'=16] {'ep'}, dimensions={1}, use_global_device_ids=true | all-gather | bytes 69632 | tf_op jit(solution)/shard_map/all_gather | solution.py:116
  51.2 2.7 %fusion.4 = f32[12,704]{1,0:T(8,128)S(1)} fusion(bf16[12,2048]{1,0:T(8,128)(2,1)S(1)} %convolution_convert_fusion, bf16[1,704,2048]{2,1,0:T(8,128)(2,1)} %param.30), kind=kOutput, calls=%fused_computation.5 | convolution fusion | flops 34603008 | bytes 2966528 | tf_op jit(solution)/shard_map/dot_general | solution.py:13
  53.9 3.5 %fusion.9 = bf16[1,12,2048]{2,1,0:T(8,128)(2,1)S(1)} fusion(bf16[1,704,2048]{2,1,0:T(8,128)(2,1)S(1)} %copy-done, bf16[12,2048]{1,0:T(8,128)(2,1)S(1)} %convolution_convert_fusion, bf16[1,704,2048]{2,1,0:T(8,128)(2,1)} %param.31, f32[12,704]{1,0:T(8,128)S(1)} %fusion.4), kind=kOutput, calls=%fused_computation.9 | convolution fusion | flops 69281280 | bytes 5899264 | tf_op jit(solution)/shard_map/dot_general | solution.py:132
  57.4 0.6 constant_dynamic-update-slice_fusion.15
  58.0 0.6 constant_dynamic-update-slice_fusion.14
  58.6 0.6 constant_dynamic-update-slice_fusion.13
  59.2 0.6 constant_dynamic-update-slice_fusion.12
  59.8 0.6 constant_dynamic-update-slice_fusion.11
  60.4 0.6 constant_dynamic-update-slice_fusion.10
  61.0 0.6 constant_dynamic-update-slice_fusion.9
  61.6 0.6 constant_dynamic-update-slice_fusion.8
  62.2 0.6 constant_dynamic-update-slice_fusion.7
  62.7 0.6 constant_dynamic-update-slice_fusion.6
  63.3 0.6 constant_dynamic-update-slice_fusion.5
  63.9 0.6 constant_dynamic-update-slice_fusion.4
  64.5 0.6 constant_dynamic-update-slice_fusion.3
  65.1 0.6 constant_dynamic-update-slice_fusion.2
  65.7 0.6 constant_dynamic-update-slice_fusion.1
  66.3 0.6 constant_dynamic-update-slice_fusion
  66.9 3.5 %all-to-all-start = ((bf16[16,1,12,128]{3,2,1,0:T(8,128)(2,1)}), bf16[16,1,12,128]{3,2,1,0:T(8,128)(2,1)S(1)}, u32[]{:S(2)}, u32[]{:S(2)}) async-start(bf16[16,1,12,128]{3,2,1,0:T(8,128)(2,1)} %constant_dynamic-update-slice_fusion), calls=%async_computation | async-start | bytes 131072 | tf_op jit(solution)/shard_map/all_to_all | solution.py:136
  70.5 1.2 %fusion.56 = f32[16,88]{1,0:T(8,128)S(1)} fusion(bf16[88,2048]{1,0:T(8,128)(2,1)} %param.33, bf16[16,2048]{1,0:T(8,128)(2,1)S(1)} %all_gather.10, f32[2048]{0:T(1024)S(1)} %copy-done.3, f32[16]{0:T(128)S(1)} %add_rsqrt_fusion), kind=kOutput, calls=%fused_computation.108 | convolution fusion | flops 5898240 | bytes 439872 | tf_op jit(solution)/shard_map/dot_general | solution.py:13
  71.8 0.3 fusion.25
  72.0 21.8 %all-gather.1 = bf16[16,88,16]{1,2,0:T(8,128)(2,1)S(1)} all-gather(bf16[1,88,16]{1,2,0:T(8,128)(2,1)S(1)} %fusion.25), channel_id=1, replica_groups=mesh['grp'=2,'ep'=16] {'ep'}, dimensions={0}, use_global_device_ids=true | all-gather | bytes 47872 | tf_op jit(solution)/shard_map/all_gather | solution.py:155
  94.2 1.2 %fusion.60 = f32[16,128]{1,0:T(8,128)S(1)} fusion(bf16[1408,16]{0,1:T(8,128)(2,1)S(1)} %reshape.352, bf16[1408,128]{1,0:T(8,128)(2,1)} %param.35), kind=kOutput, calls=%fused_computation.110 | convolution fusion | flops 5767168 | bytes 413696 | tf_op jit(solution)/shard_map/dot_general | solution.py:154
  95.6 0.8 fusion.23
  (55 shorter events, 2.2 us)
Async XLA Ops:
  0.0 53.8 %copy-start = (bf16[1,704,2048]{2,1,0:T(8,128)(2,1)S(1)}, bf16[1,704,2048]{2,1,0:T(8,128)(2,1)}, u32[]{:S(2)}) copy-start(bf16[1,704,2048]{2,1,0:T(8,128)(2,1)} %param.32) | copy-start | bytes 8650756
  0.0 7.3 %copy-start.7 = (bf16[1,2,128]{2,1,0:T(2,128)(2,1)S(1)}, bf16[1,2,128]{2,1,0:T(2,128)(2,1)}, u32[]{:S(2)}) copy-start(bf16[1,2,128]{2,1,0:T(2,128)(2,1)} %param.21) | copy-start | bytes 1540
  0.0 32.8 %copy-start.2 = (bf16[1024,128]{1,0:T(8,128)(2,1)S(1)}, bf16[1024,128]{1,0:T(8,128)(2,1)}, u32[]{:S(2)}) copy-start(bf16[1024,128]{1,0:T(8,128)(2,1)} %param.28) | copy-start | bytes 786436
  0.0 32.8 %copy-start.6 = (bf16[16,128]{1,0:T(8,128)(2,1)S(1)}, bf16[16,128]{1,0:T(8,128)(2,1)}, u32[]{:S(2)}) copy-start(bf16[16,128]{1,0:T(8,128)(2,1)} %param.27) | copy-start | bytes 12292
  1.1 49.5 %copy-start.4 = (s32[16,6]{0,1:T(8,128)S(1)}, s32[16,6]{0,1:T(8,128)}, u32[]{:S(2)}) copy-start(s32[16,6]{0,1:T(8,128)} %param.36) | copy-start | bytes 1156
  1.1 49.8 %copy-start.3 = (f32[2048]{0:T(1024)S(1)}, f32[2048]{0:T(1024)}, u32[]{:S(2)}) copy-start(f32[2048]{0:T(1024)} %param.29) | copy-start | bytes 24580
  53.8 17.9 %copy-start.1 = (bf16[88,2048]{1,0:T(8,128)(2,1)S(1)}, bf16[88,2048]{1,0:T(8,128)(2,1)}, u32[]{:S(2)}) copy-start(bf16[88,2048]{1,0:T(8,128)(2,1)} %param.34) | copy-start | bytes 1081348
  53.8 40.2 %copy-start.5 = (f32[16,6]{0,1:T(8,128)S(1)}, f32[16,6]{0,1:T(8,128)}, u32[]{:S(2)}) copy-start(f32[16,6]{0,1:T(8,128)} %param.37) | copy-start | bytes 1156
  66.9 28.7 %all-to-all-start = ((bf16[16,1,12,128]{3,2,1,0:T(8,128)(2,1)}), bf16[16,1,12,128]{3,2,1,0:T(8,128)(2,1)S(1)}, u32[]{:S(2)}, u32[]{:S(2)}) async-start(bf16[16,1,12,128]{3,2,1,0:T(8,128)(2,1)} %constant_dynamic-update-slice_fusion), calls=%async_computation | async-start | bytes 131072 | tf_op jit(solution)/shard_map/all_to_all | solution.py:136
